TPU v7x, 128 devices: a whole 4x4x4 slice. The times are simulated.
128 devices in a mesh: sp: 64 (over z, y, x), tp: 2 (over core).
Axes of the slice: x: 4, y: 4, z: 4, core: 2. Of those that a mesh axis runs over, the one named last changes fastest.
Arguments:
- residual: bfloat16 [16384, 2048], P(('sp', 'tp')), may hold values from -6 to 6
- projected: bfloat16 [16384, 2048], P('sp', 'tp'), may hold values from -6 to 6
- group_weight: bfloat16 [4, 512, 512], P('tp'), may hold values from -0.25 to 0.25
- channel_scale: float32 [2048], P('tp'), may hold values from 0.1 to 1.9
- out_weight: bfloat16 [2048, 2048], replicated, may hold values from -0.125 to 0.125
- post_mix_gain: float32 [2048], replicated, may hold values from 0.1 to 1.9
- pre_ffn_gain: float32 [2048], replicated, may hold values from 0.1 to 1.9
- post_ffn_gain: float32 [2048], replicated, may hold values from 0.1 to 1.9
- route_ids: int32 [16384, 2], P(('sp', 'tp')), may hold values from 0 to 31, all different within a row; in each aligned block of 128 rows (0 to 127, 128 to 255, ...) at most 16 rows name the same one
- route_weight: float32 [16384, 2], P(('sp', 'tp')), may hold values from 0.1 to 1
- expert_gate: bfloat16 [64, 2048, 1792], P('sp', None, 'tp'), may hold values from -0.125 to 0.125
- expert_up: bfloat16 [64, 2048, 1792], P('sp', None, 'tp'), may hold values from -0.125 to 0.125
- expert_down: bfloat16 [64, 1792, 2048], P('sp', 'tp'), may hold values from -0.09375 to 0.09375
Outputs:
- layer_out: bfloat16 [16384, 2048], P(('sp', 'tp'))
Inputs may be any that keep to these rules, and one draw needn't show every extreme that they name: `route_ids`: each row names 2 different experts. In every aligned block of 128 rows (the rows of one device) no expert is named more than 16 times, a bound that some blocks reach.
All inputs are finite; a program needn't handle non-finite values.
Results may differ from a plain program's by a relative error of at most 0.014.
Values may be sent and summed in bfloat16 or wider, within the bound.
A program may use at most 192 MiB of HBM per device.

v0:
```python
import jax
import jax.numpy as jnp
from jax import lax
from jax.sharding import PartitionSpec as P

GROUPS = 4
TOP = 2


EPS = 1e-06


def shifted(block, axis, distance):
    devices = range(lax.axis_size(axis))
    route = [(i - distance, i) for i in devices if i - distance in devices]
    return lax.ppermute(block, axis, route)


def side_by_side(arrays, axis, dim, along):
    both = jnp.concatenate(arrays, axis=along)
    whole, at, done = (lax.all_gather(both, axis, axis=dim, tiled=True), 0, [])
    for a in arrays:
        done.append(lax.slice_in_dim(whole, at, at + a.shape[along], axis=along))
        at += a.shape[along]
    return tuple(done)


def rms_scale(values, gain):
    values = values.astype(jnp.float32)
    inverse = lax.rsqrt(jnp.mean(values * values, axis=-1, keepdims=True) + EPS)
    return values * inverse * gain


def window_sums(extended, lookback, count):
    levels = []
    current = extended
    window_span = 1
    for level_id in range(GROUPS):
        current = current[window_span:] + current[:-window_span]
        window_span = window_span * 2
        first = lookback - window_span + 1
        levels.append(lax.slice_in_dim(current, first, first + count, axis=0))
    return levels


def expert_whole_half(token_rows, gate_full, up_full, down_full, parts):
    flat_rows = token_rows.reshape(-1, token_rows.shape[-1])
    quarter = gate_full.shape[1] // parts
    total = jnp.zeros(flat_rows.shape, jnp.float32)
    for part_id in range(parts):
        low = part_id * quarter
        gate_value = jnp.dot(
            flat_rows, gate_full[:, low : low + quarter], preferred_element_type=jnp.float32
        )
        up_value = jnp.dot(
            flat_rows, up_full[:, low : low + quarter], preferred_element_type=jnp.float32
        )
        active = (jax.nn.silu(gate_value) * up_value).astype(jnp.bfloat16)
        term = jnp.dot(
            active, down_full[low : low + quarter], preferred_element_type=jnp.float32
        ).astype(jnp.bfloat16)
        total = total + term.astype(jnp.float32)
    return total.astype(jnp.bfloat16).reshape(token_rows.shape)


def body(
    residual,
    projected,
    group_weight,
    channel_scale,
    out_weight,
    post_mix_gain,
    pre_ffn_gain,
    post_ffn_gain,
    route_ids,
    route_weight,
    expert_gate,
    expert_up,
    expert_down,
):
    lookback = 2**GROUPS
    tokens_here = projected.shape[0]
    width_here = projected.shape[1]
    model_width = out_weight.shape[1]
    tp_count = lax.axis_size("tp")
    tp_index = lax.axis_index("tp")
    groups_here = GROUPS // tp_count
    group_width = width_here // groups_here
    earlier = shifted(projected[tokens_here - lookback :], "sp", 1)
    extended = jnp.concatenate([earlier, projected], 0).astype(jnp.float32)
    levels = window_sums(extended, lookback, tokens_here)
    offset = lax.axis_index("sp") * tokens_here
    position = (offset + lax.iota(jnp.int32, tokens_here) + 1).astype(jnp.float32)[:, None]
    pieces = []
    for local_group in range(groups_here):
        group_id = tp_index * groups_here + local_group
        low = local_group * group_width
        summed = jnp.zeros((tokens_here, group_width), jnp.float32)
        window_span = jnp.float32(1.0)
        for level_id in range(GROUPS):
            summed = jnp.where(
                group_id == level_id, levels[level_id][:, low : low + group_width], summed
            )
            window_span = jnp.where(
                group_id == level_id, jnp.float32(2.0 ** (level_id + 1)), window_span
            )
        own_part = projected[:, low : low + group_width].astype(jnp.float32)
        pieces.append(summed / jnp.minimum(position, window_span) - own_part)
    pooled = jnp.concatenate(pieces, 1).astype(jnp.bfloat16)
    grouped = jnp.einsum(
        "tgc,gce->tge",
        pooled.reshape(tokens_here, groups_here, group_width),
        group_weight,
        preferred_element_type=jnp.float32,
    )
    scaled = (grouped.reshape(tokens_here, width_here) * channel_scale).astype(jnp.bfloat16)
    token_major = lax.all_to_all(scaled, "tp", split_axis=0, concat_axis=1, tiled=True)
    projection = jnp.dot(token_major, out_weight, preferred_element_type=jnp.float32)
    mixed = projection.astype(jnp.bfloat16)
    middle = (residual.astype(jnp.float32) + rms_scale(mixed, post_mix_gain)).astype(jnp.bfloat16)
    normed = rms_scale(middle, pre_ffn_gain).astype(jnp.bfloat16)
    row_count = normed.shape[0]
    experts_all = lax.axis_size("sp") // 2
    capacity = 2 * TOP * row_count // experts_all
    flat_ids = route_ids.reshape(-1)
    onehot = (flat_ids[:, None] == lax.iota(jnp.int32, experts_all)[None, :]).astype(jnp.int32)
    before = jnp.cumsum(onehot, 0) - onehot
    slot_ids = jnp.sum(before * onehot, 1)
    target = flat_ids * capacity + slot_ids
    source_row = lax.iota(jnp.int32, row_count * TOP) // TOP + 1
    source = jnp.zeros((experts_all * capacity,), jnp.int32).at[target].set(source_row)
    filled = source > 0
    table = jnp.where(
        filled[:, None], normed[jnp.maximum(source - 1, 0)], jnp.zeros((), jnp.bfloat16)
    )
    gate_part = expert_gate[0]
    up_part = expert_up[0]
    down_part = expert_down[0]
    gate_full, up_full = side_by_side((gate_part, up_part), "tp", 1, 0)
    down_full = lax.all_gather(down_part, "tp", axis=0, tiled=True)
    send_rows = jnp.repeat(table.reshape(experts_all, capacity, model_width), 2, axis=0)
    summed_half = expert_whole_half(
        lax.all_to_all(send_rows, "sp", split_axis=0, concat_axis=0, tiled=True),
        gate_full,
        up_full,
        down_full,
        tp_count,
    )
    returned = lax.all_to_all(summed_half, "sp", split_axis=0, concat_axis=0, tiled=True)
    pairs = returned.astype(jnp.float32).reshape(experts_all, 2, capacity, model_width)
    results = lax.optimization_barrier((pairs[:, 0] + pairs[:, 1]).astype(jnp.bfloat16))
    picked = results.reshape(experts_all * capacity, model_width)[target].astype(jnp.float32)
    weighted = picked * route_weight.reshape(-1)[:, None]
    ffn_sum = jnp.sum(weighted.reshape(row_count, TOP, model_width), 1)
    return (middle.astype(jnp.float32) + rms_scale(ffn_sum, post_ffn_gain)).astype(jnp.bfloat16)


def solution(mesh):
    in_specs = (
        P(("sp", "tp"), None),
        P("sp", "tp"),
        P("tp", None, None),
        P("tp"),
        P(),
        P(),
        P(),
        P(),
        P(("sp", "tp"), None),
        P(("sp", "tp"), None),
        P("sp", None, "tp"),
        P("sp", None, "tp"),
        P("sp", "tp", None),
    )
    out_specs = P(("sp", "tp"), None)
    return jax.shard_map(body, mesh=mesh, in_specs=in_specs, out_specs=out_specs, check_vma=False)
```

profile of v0, /device:TPU:0, one launch (start us, length us, event | category | flops | bytes accessed | tf_op | source)
XLA Modules:
  0.0 234.0 jit_solution(6956599920588247006)
XLA Ops:
  6.5 0.0 copy-start
  6.5 6.8 %pad_maximum_fusion = bf16[4096,896]{1,0:T(8,128)(2,1)} fusion(bf16[2048,896]{1,0:T(8,128)(2,1)} %bitcast.73, bf16[2048,896]{1,0:T(8,128)(2,1)} %bitcast.74), kind=kLoop, calls=%fused_computation.4 | loop fusion | flops 14680064 | bytes 14680064 | tf_op jit(solution)/shard_map/concatenate | solution.py:20
  13.3 0.0 all-gather.4.cloned.1.call-update
  13.4 1.0 copy-done.4
  14.4 3.5 %collective-permute-start = (bf16[16,1024]{1,0:T(8,128)(2,1)S(1)}, bf16[16,1024]{1,0:T(8,128)(2,1)S(1)}, u32[]{:S(2)}, u32[]{:S(2)}) collective-permute-start(bf16[16,1024]{1,0:T(8,128)(2,1)S(1)} %slice.105), channel_id=1, source_target_pairs={{0,2},{2,4},{4,6},{6,8},{8,10},{10,12},{12,14},{14,16},{16,18},{18... | collective-permute-start | bytes 98312 | tf_op jit(solution)/shard_map/ppermute | solution.py:16
  17.9 0.1 copy.20
  18.0 0.1 eq.69
  18.2 0.1 eq.65
  18.3 0.6 reduce-window.6
  18.9 0.2 slice_reduce_fusion
  19.2 0.1 copy.19
  19.3 0.1 mul.125
  19.5 0.1 fusion.40
  19.6 1.4 scatter_custom_fusion
  21.0 0.1 broadcast_in_dim.18
  21.1 0.0 collective-permute-done
  21.1 0.1 maximum_convert_fusion
  21.2 0.2 slice_add_fusion.2
  21.4 0.2 slice_add_fusion.1
  21.6 0.2 slice_add_fusion
  21.8 0.1 slice_add_fusion.3
  22.0 0.3 fusion.36
  22.3 0.3 fusion.37
  22.6 0.0 copy-start.9
  22.6 0.4 convolution_bitcast_fusion
  23.0 0.8 copy.17
  23.9 0.9 reshape.141
  24.8 0.0 copy-done.9
  24.8 0.1 multiply_convert_fusion.2
  24.9 4.2 %all_to_all.26 = bf16[2,128,1024]{2,1,0:T(8,128)(2,1)S(1)} all-to-all(bf16[2,128,1024]{2,1,0:T(8,128)(2,1)S(1)} %multiply_convert_fusion.2), channel_id=1, replica_groups=mesh['sp'=64,'tp'=2] {'tp'}, dimensions={0} | all-to-all | bytes 1048576 | tf_op jit(solution)/shard_map/all_to_all | solution.py:117
  29.0 0.3 copy.18
  29.3 0.0 copy-start.5
  29.3 0.0 copy-start.6
  29.3 0.0 copy-start.7
  29.3 6.6 %multiply_reduce_fusion.2 = (f32[128]{0:T(128)S(1)}, f32[128,2048]{1,0:T(8,128)S(1)}) fusion(bf16[128,2048]{0,1:T(8,128)(2,1)S(1)} %bitcast.75, bf16[2048,2048]{1,0:T(8,128)(2,1)} %param.17), kind=kOutput, calls=%fused_computation.41 | convolution fusion | flops 1074790272 | bytes 9961984 | tf_op jit(solution)/shard_map/dot_general | solution.py:118
  36.0 0.0 copy-done.5
  36.0 0.0 copy-done.6
  36.0 0.4 fusion.17
  36.4 0.0 copy-done.7
  36.4 0.2 fusion.19
  36.6 2.5 %gather_fusion = bf16[512,2048]{1,0:T(8,128)(2,1)S(1)} fusion(bf16[128,2048]{1,0:T(8,128)(2,1)S(1)} %fusion.19, s32[1024]{0:T(1024)S(1)} %pad_clamp_fusion.1), kind=kCustom, calls=%fused_computation | custom fusion | bytes 4196352 | tf_op jit(solution)/shard_map/gather | solution.py:134
  39.1 0.2 broadcast_select_fusion
  39.3 2.6 %broadcast_in_dim.36 = bf16[32,2,16,2048]{3,2,1,0:T(8,128)(2,1)} broadcast(bf16[32,16,2048]{2,1,0:T(8,128)(2,1)S(1)} %broadcast_select_fusion), dimensions={0,2,3} | broadcast | bytes 6291456 | tf_op jit(solution)/shard_map/broadcast_in_dim | solution.py:141
  41.9 11.2 %all-to-all-start.1 = ((bf16[64,16,2048]{2,1,0:T(8,128)(2,1)}), bf16[64,16,2048]{2,1,0:T(8,128)(2,1)}, u32[]{:S(2)}, u32[]{:S(2)}) async-start(bf16[64,16,2048]{2,1,0:T(8,128)(2,1)} %bitcast.70), calls=%async_computation.1 | async-start | bytes 8388608 | tf_op jit(solution)/shard_map/all_to_all | solution.py:143
  53.1 0.2 all-gather.6.cloned.1.call-start
  53.4 0.5 all-gather.6.cloned.1.call-update
  53.9 53.6 %all-to-all-done.1 = bf16[64,16,2048]{2,1,0:T(8,128)(2,1)} async-done(((bf16[64,16,2048]{2,1,0:T(8,128)(2,1)}), bf16[64,16,2048]{2,1,0:T(8,128)(2,1)}, u32[]{:S(2)}, u32[]{:S(2)}) %all-to-all-start.1) | async-done | bytes 4194336 | tf_op jit(solution)/shard_map/all_to_all | solution.py:143
  107.5 7.5 %fusion.2 = f32[1024,896]{1,0:T(8,128)S(1)} fusion(bf16[1024,2048]{1,0:T(8,128)(2,1)} %bitcast.10, bf16[4096,1792]{1,0:T(8,128)(2,1)} %all-gather.4.cloned.1.call-done), kind=kOutput, calls=%fused_computation.10 | convolution fusion | flops 3758096384 | bytes 11534336 | tf_op jit(solution)/shard_map/dot_general | solution.py:55
  115.0 6.3 %fusion.7 = f32[1024,896]{1,0:T(8,128)S(1)} fusion(bf16[1024,2048]{1,0:T(8,128)(2,1)} %bitcast.10, bf16[4096,1792]{1,0:T(8,128)(2,1)S(1)} %copy-done.12), kind=kOutput, calls=%fused_computation.16 | convolution fusion | flops 3758096384 | bytes 11534336 | tf_op jit(solution)/shard_map/dot_general | solution.py:55
  121.3 7.0 %multiply_convert_fusion = bf16[1024,896]{1,0:T(8,128)(2,1)S(1)} fusion(f32[1024,896]{1,0:T(8,128)S(1)} %fusion.2, bf16[1024,2048]{1,0:T(8,128)(2,1)} %bitcast.10, bf16[4096,1792]{1,0:T(8,128)(2,1)S(1)} %copy-done.12), kind=kOutput, calls=%fused_computation.20 | convolution fusion | flops 3763601408 | bytes 13369344 | tf_op jit(solution)/shard_map/dot_general | solution.py:52
  128.3 8.5 %multiply_convert_fusion.1 = bf16[1024,896]{1,0:T(8,128)(2,1)} fusion(f32[1024,896]{1,0:T(8,128)S(1)} %fusion.7, bf16[1024,2048]{1,0:T(8,128)(2,1)} %bitcast.10, bf16[4096,1792]{1,0:T(8,128)(2,1)S(1)} %copy-done.12), kind=kOutput, calls=%fused_computation.21 | convolution fusion | flops 3763601408 | bytes 13369344 | tf_op jit(solution)/shard_map/dot_general | solution.py:52
  136.8 7.2 %fusion.6 = bf16[1024,2048]{1,0:T(8,128)(2,1)S(1)} fusion(bf16[1024,896]{1,0:T(8,128)(2,1)} %multiply_convert_fusion.1, bf16[1,1792,2048]{2,1,0:T(8,128)(2,1)} %all-gather.6.cloned.1.call-done), kind=kOutput, calls=%fused_computation.15 | convolution fusion | flops 3758096384 | bytes 9699328 | tf_op jit(solution)/shard_map/dot_general | solution.py:59
  144.0 6.3 %add_convert_fusion = bf16[1024,2048]{1,0:T(8,128)(2,1)} fusion(bf16[1024,2048]{1,0:T(8,128)(2,1)S(1)} %fusion.6, bf16[1024,896]{1,0:T(8,128)(2,1)S(1)} %multiply_convert_fusion, bf16[1,1792,2048]{2,1,0:T(8,128)(2,1)S(1)} %copy-done.13), kind=kOutput, calls=%fused_computation.3 | convolution fusion | flops 3768582144 | bytes 13893632 | tf_op jit(solution)/shard_map/dot_general | solution.py:59
  150.3 9.5 %all-to-all-start.2 = ((bf16[64,16,2048]{2,1,0:T(8,128)(2,1)}), bf16[64,16,2048]{2,1,0:T(8,128)(2,1)}, u32[]{:S(2)}, u32[]{:S(2)}) async-start(bf16[64,16,2048]{2,1,0:T(8,128)(2,1)} %bitcast.72), calls=%async_computation.2 | async-start | bytes 8388608 | tf_op jit(solution)/shard_map/all_to_all | solution.py:149
  159.9 0.1 copy.25
  160.0 54.0 %all-to-all-done.2 = bf16[64,16,2048]{2,1,0:T(8,128)(2,1)} async-done(((bf16[64,16,2048]{2,1,0:T(8,128)(2,1)}), bf16[64,16,2048]{2,1,0:T(8,128)(2,1)}, u32[]{:S(2)}, u32[]{:S(2)}) %all-to-all-start.2) | async-done | bytes 4194336 | tf_op jit(solution)/shard_map/all_to_all | solution.py:149
  214.0 3.3 %convert.12 = f32[32,2,16,2048]{3,2,1,0:T(8,128)S(1)} convert(bf16[32,2,16,2048]{3,2,1,0:T(8,128)(2,1)} %bitcast.17) | non-fusion elementwise | flops 2097152 | bytes 12582912 | tf_op jit(solution)/shard_map/reshape | solution.py:150
  217.3 0.6 fusion.16
  217.9 2.3 gather_fusion.1
  220.3 2.5 %reshape.151 = f32[128,2,2048]{2,1,0:T(2,128)S(1)} reshape(bf16[256,2048]{1,0:T(8,128)(2,1)} %gather_fusion.1) | data formatting | bytes 3145728 | tf_op jit(solution)/shard_map/convert_element_type | solution.py:152
  222.7 0.0 copy-start.3
  222.8 3.2 %multiply_reduce_fusion = f32[128,2048]{1,0:T(8,128)S(1)} fusion(f32[128,2,2048]{2,1,0:T(2,128)S(1)} %reshape.151, f32[128,2]{1,0:T(8,128)S(1)} %copy.25), kind=kLoop, calls=%fused_computation.25 | loop fusion | flops 786432 | bytes 3146752 | tf_op jit(solution)/shard_map/reduce_sum | solution.py:154
  225.9 0.2 multiply_reduce_fusion.1
  226.1 1.0 fusion.20
  (35 shorter events, 0.2 us)
Async XLA Ops:
  6.5 16.0 %copy-start = (bf16[2,512,512]{2,1,0:T(8,128)(2,1)S(1)}, bf16[2,512,512]{2,1,0:T(8,128)(2,1)}, u32[]{:S(2)}) copy-start(bf16[2,512,512]{2,1,0:T(8,128)(2,1)} %param.15) | copy-start | bytes 3145732
  6.5 100.9 %all-gather.4.cloned.1.call-start = ((), (), s32[]{:S(2)}) async-start(), calls=%async_computation.3 | async-start | bytes 22020096 | tf_op jit(solution)/shard_map/all_gather | solution.py:21
  13.3 1.0 copy-start.4
  13.3 4.6 %copy-start.10 = (s32[128,2]{0,1:T(2,128)S(1)}, s32[128,2]{0,1:T(2,128)}, u32[]{:S(2)}) copy-start(s32[128,2]{0,1:T(2,128)} %param.21) | copy-start | bytes 3076
  14.4 6.8 %collective-permute-start = (bf16[16,1024]{1,0:T(8,128)(2,1)S(1)}, bf16[16,1024]{1,0:T(8,128)(2,1)S(1)}, u32[]{:S(2)}, u32[]{:S(2)}) collective-permute-start(bf16[16,1024]{1,0:T(8,128)(2,1)S(1)} %slice.105), channel_id=1, source_target_pairs={{0,2},{2,4},{4,6},{6,8},{8,10},{10,12},{12,14},{14,16},{16,18},{18... | collective-permute-start | bytes 98312 | tf_op jit(solution)/shard_map/ppermute | solution.py:16
  22.6 2.2 copy-start.9
  29.3 6.7 %copy-start.5 = (bf16[128,2048]{1,0:T(8,128)(2,1)S(1)}, bf16[128,2048]{1,0:T(8,128)(2,1)}, u32[]{:S(2)}) copy-start(bf16[128,2048]{1,0:T(8,128)(2,1)} %param.13) | copy-start | bytes 1572868
  29.3 6.7 %copy-start.6 = (f32[2048]{0:T(1024)S(1)}, f32[2048]{0:T(1024)}, u32[]{:S(2)}) copy-start(f32[2048]{0:T(1024)} %param.18) | copy-start | bytes 24580
  29.3 7.1 %copy-start.7 = (f32[2048]{0:T(1024)S(1)}, f32[2048]{0:T(1024)}, u32[]{:S(2)}) copy-start(f32[2048]{0:T(1024)} %param.19) | copy-start | bytes 24580
  36.4 2.7 %copy-start.2 = (bf16[128,2048]{1,0:T(8,128)(2,1)}, bf16[128,2048]{1,0:T(8,128)(2,1)S(1)}, u32[]{:S(2)}) copy-start(bf16[128,2048]{1,0:T(8,128)(2,1)S(1)} %get-tuple-element.6) | copy-start | bytes 1572868
  41.9 65.6 %all-to-all-start.1 = ((bf16[64,16,2048]{2,1,0:T(8,128)(2,1)}), bf16[64,16,2048]{2,1,0:T(8,128)(2,1)}, u32[]{:S(2)}, u32[]{:S(2)}) async-start(bf16[64,16,2048]{2,1,0:T(8,128)(2,1)} %bitcast.70), calls=%async_computation.1 | async-start | bytes 8388608 | tf_op jit(solution)/shard_map/all_to_all | solution.py:143
  53.1 83.6 %all-gather.6.cloned.1.call-start = ((), (), s32[]{:S(2)}) async-start(), calls=%async_computation.4 | async-start | bytes 11010048 | tf_op jit(solution)/shard_map/all_gather | solution.py:140
  107.5 7.5 %copy-start.12 = (bf16[4096,1792]{1,0:T(8,128)(2,1)S(1)}, bf16[4096,1792]{1,0:T(8,128)(2,1)}, u32[]{:S(2)}) copy-start(bf16[4096,1792]{1,0:T(8,128)(2,1)} %all-gather.4.cloned.1.call-done) | copy-start | bytes 44040196
  136.8 7.2 %copy-start.13 = (bf16[1,1792,2048]{2,1,0:T(8,128)(2,1)S(1)}, bf16[1,1792,2048]{2,1,0:T(8,128)(2,1)}, u32[]{:S(2)}) copy-start(bf16[1,1792,2048]{2,1,0:T(8,128)(2,1)} %all-gather.6.cloned.1.call-done) | copy-start | bytes 22020100
  150.3 9.6 %copy-start.11 = (f32[128,2]{0,1:T(2,128)S(1)}, f32[128,2]{0,1:T(2,128)}, u32[]{:S(2)}) copy-start(f32[128,2]{0,1:T(2,128)} %param.22) | copy-start | bytes 3076
  150.3 63.7 %all-to-all-start.2 = ((bf16[64,16,2048]{2,1,0:T(8,128)(2,1)}), bf16[64,16,2048]{2,1,0:T(8,128)(2,1)}, u32[]{:S(2)}, u32[]{:S(2)}) async-start(bf16[64,16,2048]{2,1,0:T(8,128)(2,1)} %bitcast.72), calls=%async_computation.2 | async-start | bytes 8388608 | tf_op jit(solution)/shard_map/all_to_all | solution.py:149
  220.3 5.8 %copy-start.8 = (f32[2048]{0:T(1024)S(1)}, f32[2048]{0:T(1024)}, u32[]{:S(2)}) copy-start(f32[2048]{0:T(1024)} %param.20) | copy-start | bytes 24580
  220.3 6.9 %copy-start.1 = (bf16[2,512,512]{2,1,0:T(8,128)(2,1)S(1)}, bf16[2,512,512]{2,1,0:T(8,128)(2,1)}, u32[]{:S(2)}) copy-start(bf16[2,512,512]{2,1,0:T(8,128)(2,1)} %param.15) | copy-start | bytes 3145732
  222.7 3.4 %copy-start.3 = (bf16[128,2048]{1,0:T(8,128)(2,1)S(1)}, bf16[128,2048]{1,0:T(8,128)(2,1)}, u32[]{:S(2)}) copy-start(bf16[128,2048]{1,0:T(8,128)(2,1)} %copy-done.2) | copy-start | bytes 1572868
Sparse Core Ops, SparseCore 0:
  13.5 31.9 all-gather.3
  55.6 22.1 all-gather.5
where the time goes:
time: 234 us
  waiting for transfers between devices  108 us (46%)
  matrix products  49.9 us (21%)
  starting transfers between devices  24.5 us (10%)
  other arithmetic  18.1 us (8%)
  local copies, waits for them, and re-layouts  15.3 us (7%)
  between operations  13.9 us (6%)
  blocking collectives  4.15 us (2%)
    all_to_all x1, waiting for transfers between devices, body(): lax.all_to_all(summed_half, 'sp', split_axis=0, concat_axis=0, tiled=True)  54 us
    all_to_all x1, waiting for transfers between devices, body(): lax.all_to_all(send_rows, 'sp', split_axis=0, concat_axis=0, tiled=True)  53.6 us
    dot_general x2, matrix products, expert_whole_half(): jnp.dot(flat_rows, gate_full[:, low:low + quarter], preferred_element_typ...  15.5 us
    dot_general x2, matrix products, expert_whole_half(): jnp.dot(flat_rows, up_full[:, low:low + quarter], preferred_element_type=...  13.8 us
    dot_general x2, matrix products, expert_whole_half(): jnp.dot(active, down_full[low:low + quarter], preferred_element_type=jnp....  13.6 us
    all_to_all x1, starting transfers between devices, body(): lax.all_to_all(send_rows, 'sp', split_axis=0, concat_axis=0, tiled=True)  11.2 us
    all_to_all x1, starting transfers between devices, body(): lax.all_to_all(summed_half, 'sp', split_axis=0, concat_axis=0, tiled=True)  9.54 us
    concatenate x1, other arithmetic, side_by_side(): both = jnp.concatenate(arrays, axis=along)  6.78 us
  transfers between devices with their start and end apart: 5, of which 2 were waited for; matrix products, arithmetic and copies ran while one was open for 21% of the time, Pallas kernels for 0%

commit v1 on v0

v1 whole, which is shorter than its diff:
```python
import functools

import jax
import jax.numpy as jnp
from jax import lax
from jax.experimental import pallas as pl
from jax.experimental.pallas import tpu as pltpu
from jax.sharding import PartitionSpec as P

EPS = 1e-06
MESH = pl.DeviceIdType.MESH
F32 = jnp.float32
BF16 = jnp.bfloat16
SIDE = 4
WAVES = 4
TILE = 256


def dot(a, b):
    return jnp.dot(a, b, preferred_element_type=F32)


def flag(condition):
    return jnp.where(condition, 1.0, 0.0).astype(F32)


def layer(
    res_h, proj_h, gw_h, cs, ow_h, post_mix, pre_ffn, post_ffn, ids_t, ids, wts, eg_h, eu_h, ed_h,
    out,
    pbuf, gw, ow, res, scaled, token, mid, normed, pick, table, rbuf, obuf, rr, gf, uf, df, act, wcat,
    proj_acc, lsem, wsem, wrem, hsem, tsem, dsend, drecv, rsend, rrecv,
):
    sp = lax.axis_index("sp")
    tp = lax.axis_index("tp")
    other = 1 - tp
    n_sp = lax.axis_size("sp")
    z, y, x = sp // (SIDE * SIDE), (sp // SIDE) % SIDE, sp % SIDE
    rows = out.shape[0]
    width = out.shape[1]
    half_width = width // 2
    cap = table.shape[0] // (n_sp // 2)
    quarter = eg_h.shape[2]
    look = pbuf.shape[0] - 2 * rows
    per_wave = n_sp // WAVES

    def offsets(k):
        c, i = k // per_wave, k % per_wave
        dx, dy = i % SIDE, i // SIDE
        return (c + 2 * SIDE - dx - dy) % SIDE, dy, dx

    def ahead(k):
        dz, dy, dx = offsets(k)
        return ((z + dz) % SIDE) * SIDE * SIDE + ((y + dy) % SIDE) * SIDE + (x + dx) % SIDE

    def behind(k):
        dz, dy, dx = offsets(k)
        return (
            ((z + SIDE - dz) % SIDE) * SIDE * SIDE
            + ((y + SIDE - dy) % SIDE) * SIDE
            + (x + SIDE - dx) % SIDE
        )

    barrier = pltpu.get_barrier_semaphore()

    def greet(k, carry):
        pl.semaphore_signal(barrier, inc=1, device_id=(ahead(k), tp), device_id_type=MESH)
        return carry

    lax.fori_loop(1, n_sp, greet, 0)
    pl.semaphore_signal(barrier, inc=1, device_id=(sp, other), device_id_type=MESH)

    own_cols = pl.ds(pl.multiple_of(tp * quarter, 128), quarter)
    own_rows = pl.ds(pl.multiple_of(tp * quarter, 128), quarter)
    local = [
        pltpu.make_async_copy(proj_h, pbuf.at[pl.ds(look, 2 * rows)], lsem.at[0]),
        pltpu.make_async_copy(gw_h, gw, lsem.at[1]),
        pltpu.make_async_copy(ow_h, ow, lsem.at[2]),
        pltpu.make_async_copy(res_h, res, lsem.at[3]),
        pltpu.make_async_copy(eg_h.at[0], gf.at[:, own_cols], lsem.at[4]),
        pltpu.make_async_copy(eu_h.at[0], uf.at[:, own_cols], lsem.at[5]),
        pltpu.make_async_copy(ed_h.at[0], df.at[own_rows], lsem.at[6]),
    ]
    for copy in local:
        copy.start()

    experts = n_sp // 2
    e_sub = lax.broadcasted_iota(jnp.int32, (experts, rows), 0)
    named_t = flag(e_sub == ids_t[0:1, :]) + flag(e_sub == ids_t[1:2, :])
    r0 = lax.broadcasted_iota(jnp.int32, (rows, rows), 0)
    r1 = lax.broadcasted_iota(jnp.int32, (rows, rows), 1)
    before_t = dot(named_t.astype(BF16), flag(r0 < r1).astype(BF16))
    slots = experts * cap
    s0 = lax.broadcasted_iota(jnp.int32, (slots, experts), 0)
    s1 = lax.broadcasted_iota(jnp.int32, (slots, experts), 1)
    spread_t = flag(s0 // cap == s1).astype(BF16)
    named_slot = dot(spread_t, named_t.astype(BF16))
    before_slot = dot(spread_t, before_t.astype(BF16))
    place = (lax.broadcasted_iota(jnp.int32, (slots, rows), 0) % cap).astype(F32)
    pick[...] = flag((named_slot > 0.5) & (before_slot == place)).astype(BF16)

    e_lane = lax.broadcasted_iota(jnp.int32, (rows, experts), 1)
    first, second = flag(e_lane == ids[:, 0:1]), flag(e_lane == ids[:, 1:2])
    named = first + second
    before = dot(flag(r1 < r0).astype(BF16), named.astype(BF16))
    weight = first * wts[:, 0:1] + second * wts[:, 1:2]
    high = weight.astype(BF16)
    low = (weight - high.astype(F32)).astype(BF16)
    q0 = lax.broadcasted_iota(jnp.int32, (experts, 2 * slots), 0)
    q1 = lax.broadcasted_iota(jnp.int32, (experts, 2 * slots), 1)
    spread = flag(q1 // (2 * cap) == q0).astype(BF16)
    lane_place = (lax.broadcasted_iota(jnp.int32, (rows, 2 * slots), 1) % cap).astype(F32)
    here = (dot(named.astype(BF16), spread) > 0.5) & (dot(before.astype(BF16), spread) == lane_place)
    wcat[0:rows] = jnp.where(here, dot(high, spread), 0.0).astype(BF16)
    wcat[rows : 2 * rows] = jnp.where(here, dot(low, spread), 0.0).astype(BF16)

    local[0].wait()
    pl.semaphore_wait(barrier, n_sp)

    halo = pltpu.make_async_remote_copy(
        src_ref=pbuf.at[pl.ds(2 * rows, look)],
        dst_ref=pbuf.at[pl.ds(0, look)],
        send_sem=hsem.at[0],
        recv_sem=hsem.at[1],
        device_id=((sp + 1) % n_sp, tp),
        device_id_type=MESH,
    )
    halo.start()
    pushes = [
        pltpu.make_async_remote_copy(
            src_ref=src, dst_ref=dst, send_sem=wsem.at[i], recv_sem=wrem.at[i],
            device_id=(sp, other), device_id_type=MESH,
        )
        for i, (src, dst) in enumerate(
            (
                (eg_h.at[0], gf.at[:, own_cols]),
                (eu_h.at[0], uf.at[:, own_cols]),
                (ed_h.at[0], df.at[own_rows]),
            )
        )
    ]
    for push in pushes:
        push.start()

    halo.wait()
    local[1].wait()
    group = gw.shape[1]
    total = pbuf.shape[0]
    row_id = lax.broadcasted_iota(jnp.int32, (total, group), 0)
    position = (row_id - look + 1 + sp * (2 * rows)).astype(F32)
    for lg in range(2):
        cols = slice(lg * group, (lg + 1) * group)
        own = pbuf[:, cols].astype(F32)
        own = jnp.where((row_id >= look) | (sp > 0), own, 0.0)
        sums = [own]
        for level in range(4):
            sums.append(pltpu.roll(sums[-1], 2**level, 0) + sums[-1])
        summed = jnp.where(tp == 0, sums[lg + 1], sums[lg + 3])
        span = jnp.where(tp == 0, F32(2.0 ** (lg + 1)), F32(2.0 ** (lg + 3)))
        pooled = (summed / jnp.minimum(position, span) - own).astype(BF16)[look:]
        scaled[:, cols] = (dot(pooled, gw[lg]) * cs[:, cols]).astype(BF16)

    swap = pltpu.make_async_remote_copy(
        src_ref=scaled.at[pl.ds(pl.multiple_of(other * rows, rows), rows)],
        dst_ref=token,
        send_sem=tsem.at[0],
        recv_sem=tsem.at[1],
        device_id=(sp, other),
        device_id_type=MESH,
    )
    swap.start()
    local[2].wait()
    local[3].wait()
    mine = pl.ds(pl.multiple_of(tp * rows, rows), rows)

    def project(source, part, accumulate):
        def step(n, carry):
            cols = pl.ds(pl.multiple_of(n * TILE, TILE), TILE)
            block = ow[pl.ds(pl.multiple_of(part * half_width, half_width), half_width), cols]
            value = dot(source, block)
            proj_acc[:, cols] = proj_acc[:, cols] + value if accumulate else value
            return carry

        lax.fori_loop(0, width // TILE, step, 0)

    project(scaled[mine], tp, False)
    swap.wait()
    project(token[...], other, True)

    mixed = proj_acc[...].astype(BF16).astype(F32)
    inverse = lax.rsqrt(jnp.mean(mixed * mixed, axis=-1, keepdims=True) + EPS)
    middle = (res[...].astype(F32) + mixed * inverse * post_mix[...]).astype(BF16)
    mid[...] = middle
    middle = middle.astype(F32)
    inverse = lax.rsqrt(jnp.mean(middle * middle, axis=-1, keepdims=True) + EPS)
    normed[...] = (middle * inverse * pre_ffn[...]).astype(BF16)

    def fill(n, carry):
        block = pl.ds(pl.multiple_of(n * rows, rows), rows)
        table[block] = dot(pick[block], normed[...]).astype(BF16)
        return carry

    lax.fori_loop(0, slots // rows, fill, 0)

    def outgoing(k):
        peer = ahead(k)
        return pltpu.make_async_remote_copy(
            src_ref=table.at[pl.ds(pl.multiple_of((peer // 2) * cap, cap), cap)],
            dst_ref=rbuf.at[k // per_wave, pl.ds(pl.multiple_of((k % per_wave) * cap, cap), cap)],
            send_sem=dsend.at[k],
            recv_sem=drecv.at[k],
            device_id=(peer, tp),
            device_id_type=MESH,
        )

    def returning(k):
        return pltpu.make_async_remote_copy(
            src_ref=obuf.at[k // per_wave, pl.ds(pl.multiple_of((k % per_wave) * cap, cap), cap)],
            dst_ref=rr.at[pl.ds(pl.multiple_of(sp * cap, cap), cap)],
            send_sem=rsend.at[k],
            recv_sem=rrecv.at[k],
            device_id=(behind(k), tp),
            device_id_type=MESH,
        )

    def each(low, high, act_on):
        def step(k, carry):
            act_on(k)
            return carry

        lax.fori_loop(low, high, step, 0)

    each(1, n_sp, lambda k: outgoing(k).start())
    rbuf[0, 0:cap] = table[pl.ds(pl.multiple_of((sp // 2) * cap, cap), cap)]

    for copy in local[4:]:
        copy.wait()
    for push in pushes:
        push.wait()

    hidden = gf.shape[1]
    for c in range(WAVES):
        low = 1 if c == 0 else c * per_wave
        each(low, (c + 1) * per_wave, lambda k: outgoing(k).wait_recv())

        def hid(n, carry):
            cols = pl.ds(pl.multiple_of(n * TILE, TILE), TILE)
            gate = dot(rbuf[c], gf[:, cols])
            up = dot(rbuf[c], uf[:, cols])
            act[:, cols] = (jax.nn.silu(gate) * up).astype(BF16)
            return carry

        lax.fori_loop(0, hidden // TILE, hid, 0)

        def down(n, carry):
            cols = pl.ds(pl.multiple_of(n * TILE, TILE), TILE)
            obuf[c, :, cols] = dot(act[...], df[:, cols]).astype(BF16)
            return carry

        lax.fori_loop(0, width // TILE, down, 0)
        each(low, (c + 1) * per_wave, lambda k: returning(k).start())
    rr[pl.ds(pl.multiple_of(sp * cap, cap), cap)] = obuf[0, 0:cap]

    each(1, n_sp, lambda k: outgoing(k).wait_send())
    each(1, n_sp, lambda k: returning(k).wait_recv())

    def combine(n, carry):
        cols = pl.ds(pl.multiple_of(n * TILE, TILE), TILE)
        both = dot(wcat[...], rr[:, cols])
        proj_acc[:, cols] = both[0:rows] + both[rows : 2 * rows]
        return carry

    lax.fori_loop(0, width // TILE, combine, 0)
    ffn = proj_acc[...]
    inverse = lax.rsqrt(jnp.mean(ffn * ffn, axis=-1, keepdims=True) + EPS)
    out[...] = (mid[...].astype(F32) + ffn * inverse * post_ffn[...]).astype(BF16)
    each(1, n_sp, lambda k: returning(k).wait_send())


def body(
    residual, projected, group_weight, channel_scale, out_weight, post_mix_gain, pre_ffn_gain,
    post_ffn_gain, route_ids, route_weight, expert_gate, expert_up, expert_down,
):
    n_sp = lax.axis_size("sp")
    rows, width = residual.shape
    lines, local_width = projected.shape
    look = 16
    slots = n_sp // 2 * (4 * rows // (n_sp // 2))
    cap = slots // (n_sp // 2)
    quarter = expert_gate.shape[2]
    hidden = 2 * quarter
    wave_rows = n_sp // WAVES * cap
    any_, vmem = pl.BlockSpec(memory_space=pl.ANY), pl.BlockSpec(memory_space=pltpu.VMEM)
    dma = pltpu.SemaphoreType.DMA
    return pl.pallas_call(
        layer,
        name="layer",
        out_shape=jax.ShapeDtypeStruct((rows, width), BF16),
        in_specs=[any_, any_, any_, vmem, any_, vmem, vmem, vmem, vmem, vmem, vmem, any_, any_, any_],
        out_specs=vmem,
        scratch_shapes=[
            pltpu.VMEM((look + lines, local_width), BF16),
            pltpu.VMEM(group_weight.shape, BF16),
            pltpu.VMEM(out_weight.shape, BF16),
            pltpu.VMEM((rows, width), BF16),
            pltpu.VMEM((lines, local_width), BF16),
            pltpu.VMEM((rows, local_width), BF16),
            pltpu.VMEM((rows, width), BF16),
            pltpu.VMEM((rows, width), BF16),
            pltpu.VMEM((slots, rows), BF16),
            pltpu.VMEM((slots, width), BF16),
            pltpu.VMEM((WAVES, wave_rows, width), BF16),
            pltpu.VMEM((WAVES, wave_rows, width), BF16),
            pltpu.VMEM((2 * slots, width), BF16),
            pltpu.VMEM((width, hidden), BF16),
            pltpu.VMEM((width, hidden), BF16),
            pltpu.VMEM((hidden, width), BF16),
            pltpu.VMEM((wave_rows, hidden), BF16),
            pltpu.VMEM((2 * rows, 2 * slots), BF16),
            pltpu.VMEM((rows, width), F32),
            dma((7,)),
            dma((3,)),
            dma((3,)),
            dma((2,)),
            dma((2,)),
            dma((n_sp,)),
            dma((n_sp,)),
            dma((n_sp,)),
            dma((n_sp,)),
        ],
        compiler_params=pltpu.CompilerParams(
            collective_id=0, has_side_effects=True, vmem_limit_bytes=66_000_000
        ),
    )(
        residual, projected, group_weight, channel_scale.reshape(1, -1), out_weight,
        post_mix_gain.reshape(1, -1), pre_ffn_gain.reshape(1, -1), post_ffn_gain.reshape(1, -1),
        route_ids.T, route_ids, route_weight, expert_gate, expert_up, expert_down,
    )


def solution(mesh):
    in_specs = (
        P(("sp", "tp"), None),
        P("sp", "tp"),
        P("tp", None, None),
        P("tp"),
        P(),
        P(),
        P(),
        P(),
        P(("sp", "tp"), None),
        P(("sp", "tp"), None),
        P("sp", None, "tp"),
        P("sp", None, "tp"),
        P("sp", "tp", None),
    )
    out_specs = P(("sp", "tp"), None)
    return jax.shard_map(body, mesh=mesh, in_specs=in_specs, out_specs=out_specs, check_vma=False)
```

time: 234 us -> 157 us (0.67)
  the two profiles are of different devices: /device:TPU:0 before, /device:TPU:6 now
where the time goes in v1:
time: 157 us
  Pallas kernels  153 us (97%)
  local copies, waits for them, and re-layouts  4.7 us (3%)
    pallas_call x1, Pallas kernels, body(): pl.pallas_call(layer, name='layer', out_shape=jax.ShapeDtypeStruct((rows,...  153 us
    unnamed x3, local copies, waits for them, and re-layouts  4.7 us

profile of v1, /device:TPU:6, one launch (start us, length us, event | category | flops | bytes accessed | tf_op | source)
XLA Modules:
  0.0 157.2 jit_solution(7929127149471919335)
XLA Ops:
  0.0 1.4 copy.15.wts
  1.4 1.4 copy.14.ids
  2.8 152.5 %layer.1 = bf16[128,2048]{1,0:T(8,128)(2,1)} custom-call(bf16[128,2048]{1,0:T(8,128)(2,1)} %res_h.1, bf16[256,1024]{1,0:T(8,128)(2,1)} %proj_h.1, bf16[2,512,512]{2,1,0:T(8,128)(2,1)} %gw_h.1, f32[1,1024]{1,0:T(1,128)} %bitcast.8, bf16[2048,2048]{1,0:T(8,128)(2,1)} %ow_h.1, f32[1,2048]{1,0:T(1,128)} %bitcast.5, f32[1,2048]{1,0:T(1,128)} %bitcast.6, ...), custom_call_target="tpu_custom_call" | custom-call | tf_op jit(solution)/shard_map/layer/pallas_call | solution.py:294
  155.3 1.9 %copy.17 = bf16[128,2048]{1,0:T(8,128)(2,1)} copy(bf16[128,2048]{1,0:T(8,128)(2,1)} %layer.1) | data formatting | bytes 1048576

commit v2 on v1

v2 whole, which is shorter than its diff:
```python
import functools

import jax
import jax.numpy as jnp
from jax import lax
from jax.experimental import pallas as pl
from jax.experimental.pallas import tpu as pltpu
from jax.sharding import PartitionSpec as P

EPS = 1e-06
MESH = pl.DeviceIdType.MESH
F32 = jnp.float32
BF16 = jnp.bfloat16
SIDE = 4
PART = 8
TILE = 256


def dot(a, b):
    return jnp.dot(a, b, preferred_element_type=F32)


def flag(condition):
    return jnp.where(condition, 1.0, 0.0).astype(F32)


def layer(
    res_h, proj_h, gw_h, cs, ow_h, post_mix, pre_ffn, post_ffn, ids_t, wts_t, eg_h, eu_h, ed_h,
    out,
    pbuf, gw, ow, res, scaled, token, mid, normed, raw, pick, table, rbuf, obuf, hbuf, rr, gf, uf, df,
    act, wown, wcross, wpair, acc, pout, pin, ids_t2, wts_t2,
    lsem, wsem, wrem, hsem, tsem, xsend, xrecv, bsend, brecv,
):
    sp = lax.axis_index("sp")
    tp = lax.axis_index("tp")
    other = 1 - tp
    n_sp = lax.axis_size("sp")
    z, y, x = sp // (SIDE * SIDE), (sp // SIDE) % SIDE, sp % SIDE
    rows = out.shape[0]
    width = out.shape[1]
    half_width = width // 2
    cap = 4 * rows // (n_sp // 2)
    quarter = eg_h.shape[2]
    look = pbuf.shape[0] - 2 * rows
    columns = SIDE * SIDE
    slots = columns * cap
    zy = z * SIDE + y
    pair = x // 2
    facing = SIDE - 1 - x
    twin = sp + 1 - 2 * (x % 2)

    def step_of(j):
        dy = j % SIDE
        return (j // SIDE + SIDE - dy) % SIDE, dy

    def ahead(j):
        dz, dy = step_of(j)
        return ((z + dz) % SIDE) * SIDE + (y + dy) % SIDE

    def behind(j):
        dz, dy = step_of(j)
        return ((z + SIDE - dz) % SIDE) * SIDE + (y + SIDE - dy) % SIDE

    def block(j):
        return pl.ds(pl.multiple_of(j * cap, cap), cap)

    def spot(kind, j):
        if kind < 2:
            return kind, block(j)
        return 2 + j // PART, block(j % PART + PART * (kind - 2))

    def each(low, high, act_on):
        def step(k, carry):
            act_on(k)
            return carry

        lax.fori_loop(low, high, step, 0)

    def remote(src, dst, send, recv, device):
        return pltpu.make_async_remote_copy(
            src_ref=src, dst_ref=dst, send_sem=send, recv_sem=recv, device_id=device, device_id_type=MESH
        )

    barrier = pltpu.get_barrier_semaphore()

    def greet(device):
        pl.semaphore_signal(barrier, inc=1, device_id=device, device_id_type=MESH)

    each(1, columns, lambda j: greet((ahead(j) * SIDE + x, tp)))
    each(0, columns, lambda j: greet((ahead(j) * SIDE + facing, tp)))
    greet((twin, tp))
    greet((sp, other))

    own_cols = pl.ds(pl.multiple_of(tp * quarter, 128), quarter)
    own_rows = pl.ds(pl.multiple_of(tp * quarter, 128), quarter)
    local = [
        pltpu.make_async_copy(proj_h, pbuf.at[pl.ds(look, 2 * rows)], lsem.at[0]),
        pltpu.make_async_copy(gw_h, gw, lsem.at[1]),
        pltpu.make_async_copy(ow_h, ow, lsem.at[2]),
        pltpu.make_async_copy(res_h, res, lsem.at[3]),
        pltpu.make_async_copy(eg_h.at[0], gf.at[:, own_cols], lsem.at[4]),
        pltpu.make_async_copy(eu_h.at[0], uf.at[:, own_cols], lsem.at[5]),
        pltpu.make_async_copy(ed_h.at[0], df.at[own_rows], lsem.at[6]),
    ]
    for copy in local:
        copy.start()

    experts = n_sp // 2
    r0 = lax.broadcasted_iota(jnp.int32, (rows, rows), 0)
    r1 = lax.broadcasted_iota(jnp.int32, (rows, rows), 1)
    e_sub = lax.broadcasted_iota(jnp.int32, (experts, rows), 0)
    e_lane = lax.broadcasted_iota(jnp.int32, (rows, experts), 1)
    s0 = lax.broadcasted_iota(jnp.int32, (slots, experts), 0)
    s1 = lax.broadcasted_iota(jnp.int32, (slots, experts), 1)
    q0 = lax.broadcasted_iota(jnp.int32, (experts, slots), 0)
    q1 = lax.broadcasted_iota(jnp.int32, (experts, slots), 1)
    place = (lax.broadcasted_iota(jnp.int32, (slots, rows), 0) % cap).astype(F32)
    lane_place = (lax.broadcasted_iota(jnp.int32, (rows, slots), 1) % cap).astype(F32)

    def named_slots(names):
        named = flag(e_sub == names[0:1, :]) + flag(e_sub == names[1:2, :])
        return named.astype(BF16), dot(named.astype(BF16), flag(r0 < r1).astype(BF16)).astype(BF16)

    def picks(slot_info, side):
        spread = flag((s0 // cap) * 2 + side == s1).astype(BF16)
        hit = dot(spread, slot_info[0]) > 0.5
        return flag(hit & (dot(spread, slot_info[1]) == place)).astype(BF16)

    def row_info(names, values):
        sheet = [names[0:2, :].astype(F32), values[0:2, :], jnp.zeros((4, rows), F32)]
        sheet = jnp.transpose(jnp.concatenate(sheet, axis=0))
        lane = e_lane.astype(F32)
        first, second = flag(lane == sheet[:, 0:1]), flag(lane == sheet[:, 1:2])
        named = (first + second).astype(BF16)
        before = dot(flag(r1 < r0).astype(BF16), named).astype(BF16)
        weight = first * sheet[:, 2:3] + second * sheet[:, 3:4]
        high = weight.astype(BF16)
        return named, before, high, (weight - high.astype(F32)).astype(BF16)

    def weigh(ref, info, side):
        named, before, high, low = info
        spread = flag((q1 // cap) * 2 + side == q0).astype(BF16)
        here = (dot(named, spread) > 0.5) & (dot(before, spread) == lane_place)
        ref[0:rows] = jnp.where(here, dot(high, spread), 0.0).astype(BF16)
        ref[rows : 2 * rows] = jnp.where(here, dot(low, spread), 0.0).astype(BF16)

    own_slots = named_slots(ids_t)
    pick[0] = picks(own_slots, pair)
    pick[1] = picks(own_slots, 1 - pair)
    own_info = row_info(ids_t, wts_t)
    weigh(wown, own_info, pair)
    weigh(wcross, own_info, 1 - pair)

    local[0].wait()
    pl.semaphore_wait(barrier, 2 * columns + 1)
    notes = [
        remote(src, dst, bsend.at[i], brecv.at[i], (twin, tp))
        for i, (src, dst) in enumerate(((ids_t, ids_t2), (wts_t, wts_t2)))
    ]

    halo = remote(
        pbuf.at[pl.ds(2 * rows, look)], pbuf.at[pl.ds(0, look)], hsem.at[0], hsem.at[1],
        ((sp + 1) % n_sp, tp),
    )
    halo.start()
    for note in notes:
        note.start()
    pushes = [
        remote(src, dst, wsem.at[i], wrem.at[i], (sp, other))
        for i, (src, dst) in enumerate(
            (
                (eg_h.at[0], gf.at[:, own_cols]),
                (eu_h.at[0], uf.at[:, own_cols]),
                (ed_h.at[0], df.at[own_rows]),
            )
        )
    ]

    local[1].wait()
    group = gw.shape[1]

    def pool(extended, lg, start, known):
        count = extended.shape[0]
        row_id = lax.broadcasted_iota(jnp.int32, (count, group), 0)
        own = extended.astype(F32)
        if known is not None:
            own = jnp.where((row_id >= look) | known, own, 0.0)
        sums = [own]
        for level in range(4):
            sums.append(pltpu.roll(sums[-1], 2**level, 0) + sums[-1])
        summed = jnp.where(tp == 0, sums[lg + 1], sums[lg + 3])
        span = jnp.where(tp == 0, F32(2.0 ** (lg + 1)), F32(2.0 ** (lg + 3)))
        position = (row_id - look + 1 + start + sp * (2 * rows)).astype(F32)
        return (summed / jnp.minimum(position, span) - own).astype(BF16)[look:]

    def columns_of(lg):
        return slice(lg * group, (lg + 1) * group)

    for lg in range(2):
        cols = columns_of(lg)
        pooled = pool(pbuf[look:, cols], lg, look, None)
        scaled[look:, cols] = (dot(pooled, gw[lg]) * cs[:, cols]).astype(BF16)
    halo.wait()
    for lg in range(2):
        cols = columns_of(lg)
        pooled = pool(pbuf[0 : 2 * look, cols], lg, 0, sp > 0)
        scaled[0:look, cols] = (dot(pooled, gw[lg]) * cs[:, cols]).astype(BF16)

    swap = remote(
        scaled.at[pl.ds(pl.multiple_of(other * rows, rows), rows)], token, tsem.at[0], tsem.at[1],
        (sp, other),
    )
    swap.start()
    local[2].wait()
    local[3].wait()
    mine = pl.ds(pl.multiple_of(tp * rows, rows), rows)

    def project(source, part, accumulate):
        def step(n, carry):
            cols = pl.ds(pl.multiple_of(n * TILE, TILE), TILE)
            part_rows = ow[pl.ds(pl.multiple_of(part * half_width, half_width), half_width), cols]
            value = dot(source, part_rows)
            acc[:, cols] = acc[:, cols] + value if accumulate else value
            return carry

        lax.fori_loop(0, width // TILE, step, 0)

    project(scaled[mine], tp, False)
    swap.wait()
    for push in pushes:
        push.start()
    project(token[...], other, True)

    mixed = acc[...].astype(BF16).astype(F32)
    inverse = lax.rsqrt(jnp.mean(mixed * mixed, axis=-1, keepdims=True) + EPS)
    middle = (res[...].astype(F32) + mixed * inverse * post_mix[...]).astype(BF16)
    mid[...] = middle
    middle = middle.astype(F32)
    inverse = lax.rsqrt(jnp.mean(middle * middle, axis=-1, keepdims=True) + EPS)
    normed[...] = (middle * inverse * pre_ffn[...]).astype(BF16)

    raw_copy = remote(normed, raw, bsend.at[3], brecv.at[3], (twin, tp))
    raw_copy.start()

    def fill(kind, source):
        def step(n, carry):
            cols = pl.ds(pl.multiple_of(n * TILE, TILE), TILE)
            table[kind, :, cols] = dot(pick[kind], source[:, cols]).astype(BF16)
            return carry

        lax.fori_loop(0, width // TILE, step, 0)

    def outgoing(kind, j):
        peer = ahead(j)
        line = facing if kind == 2 else x
        return remote(
            table.at[(0, 2, 1)[kind], block(peer)], rbuf.at[spot(kind, j)],
            xsend.at[kind, j], xrecv.at[kind, j], (peer * SIDE + line, tp),
        )

    def pass_on(j):
        return remote(rbuf.at[spot(2, j)], rbuf.at[spot(3, j)], xsend.at[3, j], xrecv.at[3, j], (twin, tp))

    def returning(kind, j):
        line = facing if kind == 2 else x
        return remote(
            obuf.at[spot(kind, j)], rr.at[kind, block(zy)],
            xsend.at[4 + kind, j], xrecv.at[4 + kind, j], (behind(j) * SIDE + line, tp),
        )

    def halves(j):
        return remote(obuf.at[spot(3, j)], hbuf.at[block(j)], xsend.at[7, j], xrecv.at[7, j], (twin, tp))

    fill(1, normed)
    each(0, columns, lambda j: outgoing(2, j).start())
    fill(0, normed)
    each(1, columns, lambda j: outgoing(0, j).start())
    rbuf[0, 0:cap] = table[0, block(zy)]

    def relay(j):
        outgoing(2, j).wait_recv()
        pass_on(j).start()

    for note in notes:
        note.wait()
    pick[2] = picks(named_slots(ids_t2), pair)
    weigh(wpair, row_info(ids_t2, wts_t2), pair)
    each(0, PART, relay)
    raw_copy.wait_recv()
    fill(2, raw)
    each(1, columns, lambda j: outgoing(1, j).start())
    rbuf[1, 0:cap] = table[2, block(zy)]

    for copy in local[4:]:
        copy.wait()
    for push in pushes:
        push.wait()

    hidden = gf.shape[1]

    def experts_on(c, hook):
        def hid(n, carry):
            cols = pl.ds(pl.multiple_of(n * TILE, TILE), TILE)
            gate = dot(rbuf[c], gf[:, cols])
            up = dot(rbuf[c], uf[:, cols])
            act[:, cols] = (jax.nn.silu(gate) * up).astype(BF16)
            return carry

        lax.fori_loop(0, hidden // TILE, hid, 0)

        def down(n, carry):
            cols = pl.ds(pl.multiple_of(n * TILE, TILE), TILE)
            hook(n)
            obuf[c, :, cols] = dot(act[...], df[:, cols]).astype(BF16)
            return carry

        lax.fori_loop(0, width // TILE, down, 0)

    def nothing(n):
        pass

    each(1, columns, lambda j: outgoing(0, j).wait_recv())
    experts_on(0, lambda n: relay(PART + n))
    each(1, columns, lambda j: returning(0, j).start())
    rr[0, block(zy)] = obuf[0, 0:cap]

    def join(j):
        halves(j).wait_recv()
        both = obuf[spot(2, j)].astype(F32) + hbuf[block(j)].astype(F32)
        obuf[spot(2, j)] = both.astype(BF16)
        returning(2, j).start()

    each(0, PART, lambda j: pass_on(j).wait_recv())
    experts_on(2, nothing)
    each(0, PART, lambda j: halves(j).start())

    each(1, columns, lambda j: outgoing(1, j).wait_recv())
    experts_on(1, nothing)
    each(1, columns, lambda j: returning(1, j).start())
    rr[1, block(zy)] = obuf[1, 0:cap]

    each(PART, columns, lambda j: pass_on(j).wait_recv())
    experts_on(3, join)
    each(PART, columns, lambda j: halves(j).start())

    def combine(weights, kind, cols):
        both = dot(weights[...], rr[kind, :, cols])
        return both[0:rows] + both[rows : 2 * rows]

    each(1, columns, lambda j: returning(1, j).wait_recv())

    def give(n, carry):
        cols = pl.ds(pl.multiple_of(n * TILE, TILE), TILE)
        pout[:, cols] = combine(wpair, 1, cols).astype(BF16)
        return carry

    lax.fori_loop(0, width // TILE, give, 0)
    part_copy = remote(pout, pin, bsend.at[4], brecv.at[4], (twin, tp))
    part_copy.start()

    each(PART, columns, join)
    each(1, columns, lambda j: returning(0, j).wait_recv())
    each(0, columns, lambda j: returning(2, j).wait_recv())

    def gather(n, carry):
        cols = pl.ds(pl.multiple_of(n * TILE, TILE), TILE)
        acc[:, cols] = combine(wown, 0, cols) + combine(wcross, 2, cols)
        return carry

    lax.fori_loop(0, width // TILE, gather, 0)
    part_copy.wait()
    ffn = acc[...] + pin[...].astype(F32)
    inverse = lax.rsqrt(jnp.mean(ffn * ffn, axis=-1, keepdims=True) + EPS)
    out[...] = (mid[...].astype(F32) + ffn * inverse * post_ffn[...]).astype(BF16)

    raw_copy.wait_send()

    def drain(j):
        for kind in range(3):
            @pl.when((j > 0) | (kind == 2))
            def _():
                outgoing(kind, j).wait_send()
                returning(kind, j).wait_send()
        pass_on(j).wait_send()
        halves(j).wait_send()

    each(0, columns, drain)


def body(
    residual, projected, group_weight, channel_scale, out_weight, post_mix_gain, pre_ffn_gain,
    post_ffn_gain, route_ids, route_weight, expert_gate, expert_up, expert_down,
):
    n_sp = lax.axis_size("sp")
    rows, width = residual.shape
    lines, local_width = projected.shape
    look = 16
    cap = 4 * rows // (n_sp // 2)
    quarter = expert_gate.shape[2]
    hidden = 2 * quarter
    slots = SIDE * SIDE * cap
    any_, vmem = pl.BlockSpec(memory_space=pl.ANY), pl.BlockSpec(memory_space=pltpu.VMEM)
    dma = pltpu.SemaphoreType.DMA
    return pl.pallas_call(
        layer,
        name="layer",
        out_shape=jax.ShapeDtypeStruct((rows, width), BF16),
        in_specs=[any_, any_, any_, vmem, any_, vmem, vmem, vmem, vmem, vmem, any_, any_, any_],
        out_specs=vmem,
        scratch_shapes=[
            pltpu.VMEM((look + lines, local_width), BF16),
            pltpu.VMEM(group_weight.shape, BF16),
            pltpu.VMEM(out_weight.shape, BF16),
            pltpu.VMEM((rows, width), BF16),
            pltpu.VMEM((lines, local_width), BF16),
            pltpu.VMEM((rows, local_width), BF16),
            pltpu.VMEM((rows, width), BF16),
            pltpu.VMEM((rows, width), BF16),
            pltpu.VMEM((rows, width), BF16),
            pltpu.VMEM((3, slots, rows), BF16),
            pltpu.VMEM((3, slots, width), BF16),
            pltpu.VMEM((4, slots, width), BF16),
            pltpu.VMEM((4, slots, width), BF16),
            pltpu.VMEM((slots, width), BF16),
            pltpu.VMEM((3, slots, width), BF16),
            pltpu.VMEM((width, hidden), BF16),
            pltpu.VMEM((width, hidden), BF16),
            pltpu.VMEM((hidden, width), BF16),
            pltpu.VMEM((slots, hidden), BF16),
            pltpu.VMEM((2 * rows, slots), BF16),
            pltpu.VMEM((2 * rows, slots), BF16),
            pltpu.VMEM((2 * rows, slots), BF16),
            pltpu.VMEM((rows, width), F32),
            pltpu.VMEM((rows, width), BF16),
            pltpu.VMEM((rows, width), BF16),
            pltpu.VMEM((2, rows), jnp.int32),
            pltpu.VMEM((2, rows), F32),
            dma((7,)),
            dma((3,)),
            dma((3,)),
            dma((2,)),
            dma((2,)),
            dma((8, SIDE * SIDE)),
            dma((8, SIDE * SIDE)),
            dma((5,)),
            dma((5,)),
        ],
        compiler_params=pltpu.CompilerParams(
            collective_id=0, has_side_effects=True, vmem_limit_bytes=66_000_000
        ),
    )(
        residual, projected, group_weight, channel_scale.reshape(1, -1), out_weight,
        post_mix_gain.reshape(1, -1), pre_ffn_gain.reshape(1, -1), post_ffn_gain.reshape(1, -1),
        route_ids.T, route_weight.T, expert_gate, expert_up, expert_down,
    )


def solution(mesh):
    in_specs = (
        P(("sp", "tp"), None),
        P("sp", "tp"),
        P("tp", None, None),
        P("tp"),
        P(),
        P(),
        P(),
        P(),
        P(("sp", "tp"), None),
        P(("sp", "tp"), None),
        P("sp", None, "tp"),
        P("sp", None, "tp"),
        P("sp", "tp", None),
    )
    out_specs = P(("sp", "tp"), None)
    return jax.shard_map(body, mesh=mesh, in_specs=in_specs, out_specs=out_specs, check_vma=False)
```

time: 157 us -> 116 us (0.74)
  the two profiles are of different devices: /device:TPU:6 before, /device:TPU:0 now
where the time goes in v2:
time: 116 us
  Pallas kernels  114 us (98%)
  local copies, waits for them, and re-layouts  1.88 us (2%)
    pallas_call x1, Pallas kernels, body(): pl.pallas_call(layer, name='layer', out_shape=jax.ShapeDtypeStruct((rows,...  114 us

profile of v2, /device:TPU:0, one launch (start us, length us, event | category | flops | bytes accessed | tf_op | source)
XLA Modules:
  0.0 116.0 jit_solution(17834744145891806678)
XLA Ops:
  0.0 114.1 %layer.1 = bf16[128,2048]{1,0:T(8,128)(2,1)} custom-call(bf16[128,2048]{1,0:T(8,128)(2,1)} %res_h.1, bf16[256,1024]{1,0:T(8,128)(2,1)} %proj_h.1, bf16[2,512,512]{2,1,0:T(8,128)(2,1)} %gw_h.1, f32[1,1024]{1,0:T(1,128)} %bitcast.9, bf16[2048,2048]{1,0:T(8,128)(2,1)} %ow_h.1, f32[1,2048]{1,0:T(1,128)} %bitcast.6, f32[1,2048]{1,0:T(1,128)} %bitcast.7, ...), custom_call_target="tpu_custom_call" | custom-call | tf_op jit(solution)/shard_map/layer/pallas_call | solution.py:404
  114.1 1.9 %copy.15 = bf16[128,2048]{1,0:T(8,128)(2,1)} copy(bf16[128,2048]{1,0:T(8,128)(2,1)} %layer.1) | data formatting | bytes 1048576

commit v3 on v2

--- a/solution.py
+++ b/solution.py
@@ -13,6 +13,8 @@
 BF16 = jnp.bfloat16
 SIDE = 4
 PART = 8
+EARLY = 8
+JOINED = 16
 TILE = 256
 
 
@@ -67,7 +69,10 @@
     def spot(kind, j):
         if kind < 2:
             return kind, block(j)
-        return 2 + j // PART, block(j % PART + PART * (kind - 2))
+        first = PART if kind == 3 else SIDE * SIDE - PART
+        late = jnp.where(j >= first, 1, 0)
+        place = j - late * first + (kind - 2) * jnp.where(late == 1, PART, SIDE * SIDE - PART)
+        return 2 + late, block(place)
 
     def each(low, high, act_on):
         def step(k, carry):
@@ -285,7 +290,7 @@
         note.wait()
     pick[2] = picks(named_slots(ids_t2), pair)
     weigh(wpair, row_info(ids_t2, wts_t2), pair)
-    each(0, PART, relay)
+    each(0, EARLY, relay)
     raw_copy.wait_recv()
     fill(2, raw)
     each(1, columns, lambda j: outgoing(1, j).start())
@@ -297,32 +302,6 @@
         push.wait()
 
     hidden = gf.shape[1]
-
-    def experts_on(c, hook):
-        def hid(n, carry):
-            cols = pl.ds(pl.multiple_of(n * TILE, TILE), TILE)
-            gate = dot(rbuf[c], gf[:, cols])
-            up = dot(rbuf[c], uf[:, cols])
-            act[:, cols] = (jax.nn.silu(gate) * up).astype(BF16)
-            return carry
-
-        lax.fori_loop(0, hidden // TILE, hid, 0)
-
-        def down(n, carry):
-            cols = pl.ds(pl.multiple_of(n * TILE, TILE), TILE)
-            hook(n)
-            obuf[c, :, cols] = dot(act[...], df[:, cols]).astype(BF16)
-            return carry
-
-        lax.fori_loop(0, width // TILE, down, 0)
-
-    def nothing(n):
-        pass
-
-    each(1, columns, lambda j: outgoing(0, j).wait_recv())
-    experts_on(0, lambda n: relay(PART + n))
-    each(1, columns, lambda j: returning(0, j).start())
-    rr[0, block(zy)] = obuf[0, 0:cap]
 
     def join(j):
         halves(j).wait_recv()
@@ -330,23 +309,66 @@
         obuf[spot(2, j)] = both.astype(BF16)
         returning(2, j).start()
 
-    each(0, PART, lambda j: pass_on(j).wait_recv())
-    experts_on(2, nothing)
-    each(0, PART, lambda j: halves(j).start())
-
-    each(1, columns, lambda j: outgoing(1, j).wait_recv())
-    experts_on(1, nothing)
-    each(1, columns, lambda j: returning(1, j).start())
-    rr[1, block(zy)] = obuf[1, 0:cap]
-
-    each(PART, columns, lambda j: pass_on(j).wait_recv())
-    experts_on(3, join)
-    each(PART, columns, lambda j: halves(j).start())
+    some = (columns - EARLY) // 4
+
+    def expert_unit(u, carry):
+        c = (u % 2) * 2 + u // 2
+
+        @pl.when(u == 0)
+        def _():
+            each(1, columns, lambda j: outgoing(0, j).wait_recv())
+
+        @pl.when(u == 1)
+        def _():
+            each(0, PART, lambda j: pass_on(j).wait_recv())
+
+        @pl.when(u == 2)
+        def _():
+            each(1, columns, lambda j: outgoing(1, j).wait_recv())
+
+        @pl.when(u == 3)
+        def _():
+            each(PART, columns, lambda j: pass_on(j).wait_recv())
+
+        def relays(low, high):
+            @pl.when(u == 0)
+            def _():
+                each(low, high, relay)
+
+        gate = dot(rbuf[c], gf[...])
+        relays(EARLY, EARLY + some)
+        act[...] = (jax.nn.silu(gate) * dot(rbuf[c], uf[...])).astype(BF16)
+        relays(EARLY + some, EARLY + 2 * some)
+        obuf[c] = dot(act[...], df[...]).astype(BF16)
+        relays(EARLY + 2 * some, columns)
+
+        @pl.when(u == 0)
+        def _():
+            each(1, columns, lambda j: returning(0, j).start())
+            rr[0, block(zy)] = obuf[0, 0:cap]
+
+        @pl.when(u == 1)
+        def _():
+            each(0, PART, lambda j: halves(j).start())
+
+        @pl.when(u == 2)
+        def _():
+            each(1, columns, lambda j: returning(1, j).start())
+            rr[1, block(zy)] = obuf[1, 0:cap]
+
+        @pl.when(u == 3)
+        def _():
+            each(PART, columns, lambda j: halves(j).start())
+
+        return carry
+
+    lax.fori_loop(0, 4, expert_unit, 0)
 
     def combine(weights, kind, cols):
         both = dot(weights[...], rr[kind, :, cols])
         return both[0:rows] + both[rows : 2 * rows]
 
+    each(0, JOINED, join)
     each(1, columns, lambda j: returning(1, j).wait_recv())
 
     def give(n, carry):
@@ -357,8 +379,8 @@
     lax.fori_loop(0, width // TILE, give, 0)
     part_copy = remote(pout, pin, bsend.at[4], brecv.at[4], (twin, tp))
     part_copy.start()
-
-    each(PART, columns, join)
+    each(JOINED, columns, join)
+
     each(1, columns, lambda j: returning(0, j).wait_recv())
     each(0, columns, lambda j: returning(2, j).wait_recv())
 

time: 116 us -> 107 us (0.922)
  Pallas kernels: 114 us -> 105 us
    pallas_call x1, Pallas kernels: 114 us -> 105 us  [body(): pl.pallas_call(layer, name='layer', out_shape=jax.ShapeDtypeStruct((rows,...]
where the time goes in v3:
time: 107 us; the launch traced here: 106 us
  Pallas kernels  105 us (98%)
  local copies, waits for them, and re-layouts  1.88 us (2%)
    pallas_call x1, Pallas kernels, body(): pl.pallas_call(layer, name='layer', out_shape=jax.ShapeDtypeStruct((rows,...  105 us

profile of v3, /device:TPU:0, one launch (start us, length us, event | category | flops | bytes accessed | tf_op | source)
XLA Modules:
  0.0 106.5 jit_solution(14929381556592609852)
XLA Ops:
  0.0 104.6 %layer.1 = bf16[128,2048]{1,0:T(8,128)(2,1)} custom-call(bf16[128,2048]{1,0:T(8,128)(2,1)} %res_h.1, bf16[256,1024]{1,0:T(8,128)(2,1)} %proj_h.1, bf16[2,512,512]{2,1,0:T(8,128)(2,1)} %gw_h.1, f32[1,1024]{1,0:T(1,128)} %bitcast.9, bf16[2048,2048]{1,0:T(8,128)(2,1)} %ow_h.1, f32[1,2048]{1,0:T(1,128)} %bitcast.6, f32[1,2048]{1,0:T(1,128)} %bitcast.7, ...), custom_call_target="tpu_custom_call" | custom-call | tf_op jit(solution)/shard_map/layer/pallas_call | solution.py:426
  104.6 1.9 %copy.15 = bf16[128,2048]{1,0:T(8,128)(2,1)} copy(bf16[128,2048]{1,0:T(8,128)(2,1)} %layer.1) | data formatting | bytes 1048576

commit v4 on v3

--- a/solution.py
+++ b/solution.py
@@ -107,7 +107,7 @@
         pltpu.make_async_copy(eu_h.at[0], uf.at[:, own_cols], lsem.at[5]),
         pltpu.make_async_copy(ed_h.at[0], df.at[own_rows], lsem.at[6]),
     ]
-    for copy in local:
+    for copy in local[:4]:
         copy.start()
 
     experts = n_sp // 2
@@ -216,6 +216,8 @@
         (sp, other),
     )
     swap.start()
+    for copy in local[4:]:
+        copy.start()
     local[2].wait()
     local[3].wait()
     mine = pl.ds(pl.multiple_of(tp * rows, rows), rows)
@@ -232,8 +234,6 @@
 
     project(scaled[mine], tp, False)
     swap.wait()
-    for push in pushes:
-        push.start()
     project(token[...], other, True)
 
     mixed = acc[...].astype(BF16).astype(F32)
@@ -279,7 +279,9 @@
     fill(1, normed)
     each(0, columns, lambda j: outgoing(2, j).start())
     fill(0, normed)
-    each(1, columns, lambda j: outgoing(0, j).start())
+    each(1, columns, lambda j: outgoing(0, columns - j).start())
+    for push in pushes:
+        push.start()
     rbuf[0, 0:cap] = table[0, block(zy)]
 
     def relay(j):

time: 107 us -> 107 us (level)
  no operation moved by 1% of the time
where the time goes in v4:
time: 107 us; the launch traced here: 105 us
  Pallas kernels  104 us (97%)
  local copies, waits for them, and re-layouts  1.88 us (2%)
    pallas_call x1, Pallas kernels, body(): pl.pallas_call(layer, name='layer', out_shape=jax.ShapeDtypeStruct((rows,...  104 us

profile of v4, /device:TPU:0, one launch (start us, length us, event | category | flops | bytes accessed | tf_op | source)
XLA Modules:
  0.0 105.5 jit_solution(2902220571875803628)
XLA Ops:
  0.0 103.6 %layer.1 = bf16[128,2048]{1,0:T(8,128)(2,1)} custom-call(bf16[128,2048]{1,0:T(8,128)(2,1)} %res_h.1, bf16[256,1024]{1,0:T(8,128)(2,1)} %proj_h.1, bf16[2,512,512]{2,1,0:T(8,128)(2,1)} %gw_h.1, f32[1,1024]{1,0:T(1,128)} %bitcast.9, bf16[2048,2048]{1,0:T(8,128)(2,1)} %ow_h.1, f32[1,2048]{1,0:T(1,128)} %bitcast.6, f32[1,2048]{1,0:T(1,128)} %bitcast.7, ...), custom_call_target="tpu_custom_call" | custom-call | tf_op jit(solution)/shard_map/layer/pallas_call | solution.py:428
  103.6 1.9 %copy.15 = bf16[128,2048]{1,0:T(8,128)(2,1)} copy(bf16[128,2048]{1,0:T(8,128)(2,1)} %layer.1) | data formatting | bytes 1048576
